TPU v7x, 32 devices: a whole 2x2x4 slice. The times are simulated.
32 devices in a mesh: fs: 8 (over z, y), tp: 4 (over x, core).
Axes of the slice: x: 2, y: 2, z: 4, core: 2. Of those that a mesh axis runs over, the one named last changes fastest.
Arguments:
- tokens: bfloat16 [2048, 2048], P('fs', 'tp'), may hold values from -12.1 to 12.1, as said below
- gate_weight: float32 [2048, 5632], P('fs', 'tp'), may hold values from -0.125 to 0.125
- up_weight: float32 [2048, 5632], P('fs', 'tp'), may hold values from -0.125 to 0.125
- down_weight: float32 [5632, 2048], P('tp', 'fs'), may hold values from -0.078125 to 0.078125
- gate_scale: float32 [4, 1408], P('tp', 'fs'), may hold values from 0.1 to 1.9
- up_scale: float32 [4, 1408], P('tp', 'fs'), may hold values from 0.1 to 1.9
- down_scale: float32 [4, 512], P('tp', 'fs'), may hold values from 0.16 to 4.6, as said below
- bgate_weight: float32 [2048, 2048], P('fs', 'tp'), may hold values from -0.125 to 0.125
- cgate_weight: float32 [2048, 2048], P('fs', 'tp'), may hold values from -0.125 to 0.125
- value_weight: float32 [2048, 2048], P('fs', 'tp'), may hold values from -0.125 to 0.125
- bgate_scale: float32 [4, 512], P('tp', 'fs'), may hold values from 0.1 to 1.9
- cgate_scale: float32 [4, 512], P('tp', 'fs'), may hold values from 0.1 to 1.9
- value_scale: float32 [4, 512], P('tp', 'fs'), may hold values from 0.1 to 1.9
- conv_taps: float32 [3, 2048], replicated, may hold values from -3.5 to 3.5
- mixout_weight: float32 [2048, 2048], P('tp', 'fs'), may hold values from -0.125 to 0.125
- mixout_scale: float32 [4, 512], P('tp', 'fs'), may hold values from 0.16 to 4.6, as said below
- first_gain: float32 [2048], replicated, may hold values from 0.1 to 1.9
- first_shift: float32 [2048], replicated, may hold values from -1.8 to 1.8
- mixer_gain: float32 [2048], replicated, may hold values from 0.1 to 1.9
- mixer_shift: float32 [2048], replicated, may hold values from -1.8 to 1.8
- last_gain: float32 [2048], replicated, may hold values from 0.1 to 1.9
- last_shift: float32 [2048], replicated, may hold values from -1.8 to 1.8
Outputs:
- layer_out: bfloat16 [2048, 2048], P('fs', 'tp')
Inputs may be any that keep to these rules, and one draw needn't show every extreme that they name: `tokens`: normal values times one factor for each of 4 equal consecutive blocks of the features. `down_scale`: positive; one factor for each row times a spread over the columns. `mixout_scale`: positive; one factor for each row times a spread over the columns.
All inputs are finite; a program needn't handle non-finite values.
Results may differ from a plain program's by a relative error of at most 0.025.
Values may be sent and summed in bfloat16 or wider, within the bound.
No kernel may reach another device: no remote copies, remote signals or barrier semaphores. Data moves between devices by JAX's collectives and lax.ppermute only.
A program may use at most 64 MiB of HBM per device.

v0:
```python
import jax
import jax.numpy as jnp
from jax import lax
from jax.sharding import PartitionSpec as P

TAPS = 3
LENGTH = 128
RESIDUAL_SCALE = 1.4142135623730951
HALF_STEP = 0.5
EPSILON = 1e-05


def add_rows(gathered, shard_piece):
    return jnp.dot(gathered, shard_piece, preferred_element_type=jnp.float32)


def features(inputs):
    return lax.all_gather(inputs, "tp", axis=1, tiled=True)


def post_norm(residual, branch, norm_gain, norm_shift):
    summed = RESIDUAL_SCALE * residual.astype(jnp.float32) + branch
    moments = lax.psum((jnp.sum(summed, -1), jnp.sum(summed * summed, -1)), "tp")
    feature_total = summed.shape[1] * lax.axis_size("tp")
    average = (moments[0] / feature_total)[:, None]
    mean_square = (moments[1] / feature_total)[:, None]
    variance = mean_square - average * average
    return ((summed - average) * lax.rsqrt(variance + EPSILON) * norm_gain + norm_shift).astype(
        jnp.bfloat16
    )


def spread_back(weight_cols, left_rows):
    return (
        lax.psum_scatter(
            lax.dot_general(
                weight_cols, left_rows, (((0,), (1,)), ((), ())), preferred_element_type=jnp.float32
            ).astype(jnp.bfloat16),
            "tp",
            scatter_dimension=0,
            tiled=True,
        )
        .astype(jnp.float32)
        .T
    )


def shards(
    tokens,
    gate_weight,
    up_weight,
    down_weight,
    gate_scale,
    up_scale,
    down_scale,
    bgate_weight,
    cgate_weight,
    value_weight,
    bgate_scale,
    cgate_scale,
    value_scale,
    conv_taps,
    mixout_weight,
    mixout_scale,
    first_gain,
    first_shift,
    mixer_gain,
    mixer_shift,
    last_gain,
    last_shift,
):
    scales = (
        lax.all_gather(gate_scale, "fs", axis=1, tiled=True),
        lax.all_gather(up_scale, "fs", axis=1, tiled=True),
        lax.all_gather(down_scale, "fs", axis=1, tiled=True),
        lax.all_gather(bgate_scale, "fs", axis=1, tiled=True),
        lax.all_gather(cgate_scale, "fs", axis=1, tiled=True),
        lax.all_gather(value_scale, "fs", axis=1, tiled=True),
        lax.all_gather(mixout_scale, "fs", axis=1, tiled=True),
    )
    gate_cols, up_cols, down_cols, bgate_cols, cgate_cols, value_cols, mixout_cols = [
        scale_row.reshape(-1) for scale_row in scales
    ]
    tp_index = lax.axis_index("tp")
    columns = tokens.shape[1]

    def own_part(vector):
        return lax.dynamic_slice_in_dim(vector, tp_index * columns, columns)

    gate_low = gate_weight.astype(jnp.bfloat16)
    up_low = up_weight.astype(jnp.bfloat16)
    down_low = down_weight.astype(jnp.bfloat16)
    kept_gate, kept_up = (
        lax.all_gather(gate_low, "fs", axis=0, tiled=True),
        lax.all_gather(up_low, "fs", axis=0, tiled=True),
    )
    kept_down = lax.all_gather(down_low, "fs", axis=1, tiled=True)

    def channel_mix(gathered):
        gate_sum = jnp.dot(gathered, kept_gate, preferred_element_type=jnp.float32)
        up_sum = jnp.dot(gathered, kept_up, preferred_element_type=jnp.float32)
        hidden = (jax.nn.silu(gate_sum * gate_cols) * (up_sum * up_cols)).astype(jnp.bfloat16)
        return HALF_STEP * (spread_back(kept_down, hidden) * down_cols)

    first = post_norm(
        tokens, channel_mix(features(tokens)), own_part(first_gain), own_part(first_shift)
    )
    gathered = features(first)
    bgate_low = bgate_weight.astype(jnp.bfloat16)
    channels = bgate_low.shape[1]
    outgate = add_rows(gathered, lax.all_gather(bgate_low, "fs", axis=0, tiled=True))
    ingate = add_rows(
        gathered, lax.all_gather(cgate_weight.astype(jnp.bfloat16), "fs", axis=0, tiled=True)
    )
    values = add_rows(
        gathered, lax.all_gather(value_weight.astype(jnp.bfloat16), "fs", axis=0, tiled=True)
    )
    tap_weights = lax.dynamic_slice_in_dim(conv_taps, tp_index * channels, channels, 1)
    mixed = (ingate * cgate_cols * (values * value_cols)).reshape(-1, LENGTH, channels)
    padded = jnp.pad(mixed, ((0, 0), (TAPS - 1, 0), (0, 0)))
    convolved = jnp.zeros(mixed.shape, jnp.float32)
    for tap_index in range(TAPS):
        convolved = convolved + tap_weights[tap_index] * padded[:, tap_index : tap_index + LENGTH]
    gated = (outgate * bgate_cols * convolved.reshape(-1, channels)).astype(jnp.bfloat16)
    mix_full = lax.all_gather(mixout_weight.astype(jnp.bfloat16), "fs", axis=1, tiled=True)
    second = post_norm(
        first,
        spread_back(mix_full, gated) * mixout_cols,
        own_part(mixer_gain),
        own_part(mixer_shift),
    )
    return post_norm(
        second, channel_mix(features(second)), own_part(last_gain), own_part(last_shift)
    )


def solution(mesh):
    in_specs = (
        P("fs", "tp"),
        P("fs", "tp"),
        P("fs", "tp"),
        P("tp", "fs"),
        P("tp", "fs"),
        P("tp", "fs"),
        P("tp", "fs"),
        P("fs", "tp"),
        P("fs", "tp"),
        P("fs", "tp"),
        P("tp", "fs"),
        P("tp", "fs"),
        P("tp", "fs"),
        P(),
        P("tp", "fs"),
        P("tp", "fs"),
        P(),
        P(),
        P(),
        P(),
        P(),
        P(),
    )
    out_specs = P("fs", "tp")
    return jax.shard_map(shards, mesh=mesh, in_specs=in_specs, out_specs=out_specs, check_vma=False)
```

profile of v0, /device:TPU:0, one launch (start us, length us, event | category | flops | bytes accessed | tf_op | source)
XLA Modules:
  0.0 669.1 jit_solution(10766681198082173955)
XLA Ops:
  6.5 0.7 all-gather.11.cloned.1.call-update
  7.3 2.3 convert_element_type.78
  9.6 0.0 all-gather.15.cloned.1.call-start
  9.7 0.9 convert_element_type.79
  10.7 0.0 all-gather.17.cloned.1.call-start
  10.8 0.5 copy-done.5
  11.2 0.9 convert_element_type.81
  12.2 0.0 reduce-scatter.4.cloned.1.call-start
  12.3 0.6 dynamic-slice
  14.2 0.3 dynamic-update-slice
  14.5 0.3 dynamic-update-slice.1
  14.7 0.1 bitcast_dynamic-update-slice_fusion
  14.8 0.1 bitcast_dynamic-update-slice_fusion.1
  14.9 0.1 bitcast_dynamic-update-slice_fusion.2
  15.0 0.1 bitcast_dynamic-update-slice_fusion.3
  15.1 0.1 bitcast_dynamic-update-slice_fusion.4
  15.2 39.5 %all-reduce.8 = (f32[1408]{0:T(1024)S(1)}, f32[1408]{0:T(1024)S(1)}, f32[512]{0:T(512)S(1)}, f32[512]{0:T(512)S(1)}, f32[512]{0:T(512)S(1)}, /*index=5*/f32[512]{0:T(512)S(1)}, f32[512]{0:T(512)S(1)}) all-reduce(f32[1408]{0:T(1024)S(1)} %dynamic-update-slice, f32[1408]{0:T(1024)S(1)} %dynamic-update-slice.1, ...), channel_id=1, replica_groups=mesh['fs'=8,'tp'=4] {'fs'}, use_global_device_ids=true, to_apply=%add.1 | all-reduce | flops 5376 | bytes 43008
  54.7 68.3 %all-gather.13.cloned.1.call-done = bf16[2048,1408]{1,0:T(8,128)(2,1)} async-done(((bf16[256,1408]{1,0:T(8,128)(2,1)}), bf16[2048,1408]{1,0:T(8,128)(2,1)}) %all-gather.13.cloned.1.call-update) | async-done | bytes 5767184 | tf_op jit(solution)/shard_map/all_gather | solution.py:94
  123.1 4.8 convolution_multiply_fusion.3
  127.9 87.9 %all-gather.15.cloned.1.call-done = bf16[2048,1408]{1,0:T(8,128)(2,1)} async-done(((bf16[256,1408]{1,0:T(8,128)(2,1)}), bf16[2048,1408]{1,0:T(8,128)(2,1)}) %all-gather.15.cloned.1.call-update) | async-done | bytes 5767184 | tf_op jit(solution)/shard_map/all_gather | solution.py:95
  215.8 93.2 %all-gather.17.cloned.1.call-done = bf16[1408,2048]{1,0:T(8,128)(2,1)} async-done(((bf16[1408,256]{1,0:T(8,128)(2,1)}), bf16[1408,2048]{1,0:T(8,128)(2,1)}) %all-gather.17.cloned.1.call-update) | async-done | bytes 5767184 | tf_op jit(solution)/shard_map/all_gather | solution.py:97
  309.0 9.0 %fusion.4 = bf16[2048,256]{0,1:T(8,128)(2,1)} fusion(bf16[1408,2048]{1,0:T(8,128)(2,1)} %all-gather.17.cloned.1.call-done, bf16[256,2048]{1,0:T(8,128)(2,1)S(1)} %copy-done.12, bf16[2048,1408]{1,0:T(8,128)(2,1)} %all-gather.15.cloned.1.call-done, f32[256,1408]{1,0:T(8,128)S(1)} %convolution_multiply_fusion.3, f32[1408]{0:T(1024)S(1)} %get-tuple-element.12), kind=kOutput, calls=%fused_computation.11 | convolution fusion | flops 2955837440 | bytes 15078912 | tf_op jit(solution)/shard_map/dot_general | solution.py:36
  318.0 0.0 all-gather.23.cloned.1.call-start
  318.1 0.7 convert_element_type.88
  318.8 0.0 all-gather.19.cloned.1.call-start
  318.9 0.8 dynamic_slice.21
  319.7 0.8 dynamic_slice.22
  320.5 20.6 %reduce-scatter.4.cloned.1.call-done = bf16[512,256]{0,1:T(8,128)(2,1)} async-done(((bf16[2048,256]{0,1:T(8,128)(2,1)}), bf16[512,256]{0,1:T(8,128)(2,1)}) %reduce-scatter.4.cloned.1.call-update) | async-done | bytes 262160 | tf_op jit(solution)/shard_map/reduce_scatter | solution.py:35
  341.1 1.2 fusion.15
  342.3 5.8 all-reduce.11
  348.1 1.9 add_convert_fusion.2
  350.0 0.0 all-gather.25.cloned.1.call-start
  350.0 0.7 convert_element_type.89
  350.8 0.0 all-gather.21.cloned.1.call-start
  350.8 0.7 convert_element_type.87
  351.6 0.0 all-gather.27.cloned.1.call-start
  351.7 0.7 convert_element_type.91
  352.4 0.0 reduce-scatter.6.cloned.1.call-start
  352.5 0.9 constant_dynamic-slice_fusion
  353.4 38.9 %all-gather.23.cloned.1.call-done = bf16[2048,512]{1,0:T(8,128)(2,1)} async-done(((bf16[256,512]{1,0:T(8,128)(2,1)}), bf16[2048,512]{1,0:T(8,128)(2,1)}) %all-gather.23.cloned.1.call-update) | async-done | bytes 2097168 | tf_op jit(solution)/shard_map/all_gather | solution.py:113
  392.2 16.8 %all-gather.19.cloned.1.call-done = bf16[256,2048]{1,0:T(8,128)(2,1)} async-done(((bf16[256,512]{1,0:T(8,128)(2,1)}), bf16[256,2048]{1,0:T(8,128)(2,1)}) %all-gather.19.cloned.1.call-update) | async-done | bytes 1048592 | tf_op jit(solution)/shard_map/all_gather | solution.py:18
  409.0 2.7 convolution_multiply_fusion.5
  411.8 48.5 %all-gather.25.cloned.1.call-done = bf16[2048,512]{1,0:T(8,128)(2,1)} async-done(((bf16[256,512]{1,0:T(8,128)(2,1)}), bf16[2048,512]{1,0:T(8,128)(2,1)}) %all-gather.25.cloned.1.call-update) | async-done | bytes 2097168 | tf_op jit(solution)/shard_map/all_gather | solution.py:116
  460.3 2.3 fusion.7
  462.6 0.2 fusion.12
  462.8 47.3 %all-gather.21.cloned.1.call-done = bf16[2048,512]{1,0:T(8,128)(2,1)} async-done(((bf16[256,512]{1,0:T(8,128)(2,1)}), bf16[2048,512]{1,0:T(8,128)(2,1)}) %all-gather.21.cloned.1.call-update) | async-done | bytes 2097168 | tf_op jit(solution)/shard_map/all_gather | solution.py:111
  510.1 50.8 %all-gather.27.cloned.1.call-done = bf16[512,2048]{1,0:T(8,128)(2,1)} async-done(((bf16[512,256]{1,0:T(8,128)(2,1)}), bf16[512,2048]{1,0:T(8,128)(2,1)}) %all-gather.27.cloned.1.call-update) | async-done | bytes 2097168 | tf_op jit(solution)/shard_map/all_gather | solution.py:125
  560.9 4.7 fusion.6
  565.6 0.8 dynamic_slice.24
  566.4 0.8 dynamic_slice.25
  567.1 21.6 %reduce-scatter.6.cloned.1.call-done = bf16[512,256]{0,1:T(8,128)(2,1)} async-done(((bf16[2048,256]{0,1:T(8,128)(2,1)}), bf16[512,256]{0,1:T(8,128)(2,1)}) %reduce-scatter.6.cloned.1.call-update) | async-done | bytes 262160 | tf_op jit(solution)/shard_map/reduce_scatter | solution.py:35
  588.7 1.2 fusion.14
  589.9 5.8 all-reduce.10
  595.6 1.8 add_convert_fusion.1
  597.5 0.2 reduce-scatter.8.cloned.1.call-start
  597.7 17.2 %all-gather.29.cloned.1.call-done = bf16[256,2048]{1,0:T(8,128)(2,1)} async-done(((bf16[256,512]{1,0:T(8,128)(2,1)}), bf16[256,2048]{1,0:T(8,128)(2,1)}) %all-gather.29.cloned.1.call-update) | async-done | bytes 1048592 | tf_op jit(solution)/shard_map/all_gather | solution.py:18
  615.0 4.8 convolution_multiply_fusion.1
  619.8 9.0 %fusion.5 = bf16[2048,256]{0,1:T(8,128)(2,1)} fusion(bf16[1408,2048]{1,0:T(8,128)(2,1)} %all-gather.17.cloned.1.call-done, bf16[256,2048]{1,0:T(8,128)(2,1)S(1)} %copy-done.13, bf16[2048,1408]{1,0:T(8,128)(2,1)} %all-gather.15.cloned.1.call-done, f32[256,1408]{1,0:T(8,128)S(1)} %convolution_multiply_fusion.1, f32[1408]{0:T(1024)S(1)} %get-tuple-element.12), kind=kOutput, calls=%fused_computation.12 | convolution fusion | flops 2955837440 | bytes 15078912 | tf_op jit(solution)/shard_map/dot_general | solution.py:36
  628.8 0.8 dynamic_slice.26
  629.6 0.8 dynamic_slice.27
  630.4 23.4 %reduce-scatter.8.cloned.1.call-done = bf16[512,256]{0,1:T(8,128)(2,1)} async-done(((bf16[2048,256]{0,1:T(8,128)(2,1)}), bf16[512,256]{0,1:T(8,128)(2,1)}) %reduce-scatter.8.cloned.1.call-update) | async-done | bytes 262160 | tf_op jit(solution)/shard_map/reduce_scatter | solution.py:35
  653.8 1.2 fusion.16
  655.0 5.8 all-reduce.9
  660.7 1.9 add_convert_fusion
  (65 shorter events, 0.4 us)
Async XLA Ops:
  6.5 3.2 copy-start.4
  6.5 48.2 %all-gather.11.cloned.1.call-start = ((), (), s32[]{:S(2)}) async-start(), calls=%async_computation.3 | async-start | bytes 1310720 | tf_op jit(solution)/shard_map/all_gather | solution.py:18
  7.3 115.8 %all-gather.13.cloned.1.call-start = ((), (), s32[]{:S(2)}) async-start(), calls=%async_computation.4 | async-start | bytes 6488064 | tf_op jit(solution)/shard_map/all_gather | solution.py:94
  9.6 1.6 copy-start.5
  9.6 206.1 %all-gather.15.cloned.1.call-start = ((), (), s32[]{:S(2)}) async-start(), calls=%async_computation.5 | async-start | bytes 6488064 | tf_op jit(solution)/shard_map/all_gather | solution.py:95
  10.7 1.6 copy-start.19
  10.7 3.5 copy-start.10
  10.7 3.8 copy-start.11
  10.7 4.1 copy-start.14
  10.7 4.2 copy-start.15
  10.7 4.3 copy-start.16
  10.7 4.3 copy-start.17
  10.7 4.4 copy-start.18
  10.7 298.3 %all-gather.17.cloned.1.call-start = ((), (), s32[]{:S(2)}) async-start(), calls=%async_computation.6 | async-start | bytes 6488064 | tf_op jit(solution)/shard_map/all_gather | solution.py:97
  12.2 328.9 %reduce-scatter.4.cloned.1.call-start = ((), (), s32[]{:S(2)}) async-start(), calls=%async_computation.7 | async-start | bytes 1310720 | tf_op jit(solution)/shard_map/reduce_scatter | solution.py:35
  123.0 186.0 %copy-start.12 = (bf16[256,2048]{1,0:T(8,128)(2,1)S(1)}, bf16[256,2048]{1,0:T(8,128)(2,1)}, u32[]{:S(2)}) copy-start(bf16[256,2048]{1,0:T(8,128)(2,1)} %all-gather.11.cloned.1.call-done) | copy-start | bytes 3145732
  309.0 9.1 %copy-start.6 = (f32[256,512]{1,0:T(8,128)S(1)}, f32[256,512]{1,0:T(8,128)}, u32[]{:S(2)}) copy-start(f32[256,512]{1,0:T(8,128)} %param.30) | copy-start | bytes 1572868
  318.0 23.1 %copy-start.3 = (bf16[256,512]{1,0:T(8,128)(2,1)S(1)}, bf16[256,512]{1,0:T(8,128)(2,1)}, u32[]{:S(2)}) copy-start(bf16[256,512]{1,0:T(8,128)(2,1)} %param.22) | copy-start | bytes 786436
  318.0 32.0 %copy-start.7 = (f32[256,512]{1,0:T(8,128)S(1)}, f32[256,512]{1,0:T(8,128)}, u32[]{:S(2)}) copy-start(f32[256,512]{1,0:T(8,128)} %param.31) | copy-start | bytes 1572868
  318.0 32.8 %copy-start.8 = (f32[256,512]{1,0:T(8,128)S(1)}, f32[256,512]{1,0:T(8,128)}, u32[]{:S(2)}) copy-start(f32[256,512]{1,0:T(8,128)} %param.29) | copy-start | bytes 1572868
  318.0 74.2 %all-gather.23.cloned.1.call-start = ((), (), s32[]{:S(2)}) async-start(), calls=%async_computation.10 | async-start | bytes 2359296 | tf_op jit(solution)/shard_map/all_gather | solution.py:113
  318.8 32.8 %copy-start.9 = (f32[512,256]{1,0:T(8,128)S(1)}, f32[512,256]{1,0:T(8,128)}, u32[]{:S(2)}) copy-start(f32[512,256]{1,0:T(8,128)} %param.36) | copy-start | bytes 1572868
  318.8 90.2 %all-gather.19.cloned.1.call-start = ((), (), s32[]{:S(2)}) async-start(), calls=%async_computation.8 | async-start | bytes 1310720 | tf_op jit(solution)/shard_map/all_gather | solution.py:18
  350.0 110.3 %all-gather.25.cloned.1.call-start = ((), (), s32[]{:S(2)}) async-start(), calls=%async_computation.11 | async-start | bytes 2359296 | tf_op jit(solution)/shard_map/all_gather | solution.py:116
  350.8 159.3 %all-gather.21.cloned.1.call-start = ((), (), s32[]{:S(2)}) async-start(), calls=%async_computation.9 | async-start | bytes 2359296 | tf_op jit(solution)/shard_map/all_gather | solution.py:111
  351.6 209.3 %all-gather.27.cloned.1.call-start = ((), (), s32[]{:S(2)}) async-start(), calls=%async_computation.12 | async-start | bytes 2359296 | tf_op jit(solution)/shard_map/all_gather | solution.py:125
  352.4 236.3 %reduce-scatter.6.cloned.1.call-start = ((), (), s32[]{:S(2)}) async-start(), calls=%async_computation.13 | async-start | bytes 1310720 | tf_op jit(solution)/shard_map/reduce_scatter | solution.py:35
  409.0 51.2 %copy-start = (bf16[256,2048]{1,0:T(8,128)(2,1)S(1)}, bf16[256,2048]{1,0:T(8,128)(2,1)}, u32[]{:S(2)}) copy-start(bf16[256,2048]{1,0:T(8,128)(2,1)} %all-gather.19.cloned.1.call-done) | copy-start | bytes 3145732
  560.9 27.8 %copy-start.1 = (bf16[256,512]{1,0:T(8,128)(2,1)S(1)}, bf16[256,512]{1,0:T(8,128)(2,1)}, u32[]{:S(2)}) copy-start(bf16[256,512]{1,0:T(8,128)(2,1)} %add_convert_fusion.2) | copy-start | bytes 786436
  565.6 49.4 %all-gather.29.cloned.1.call-start = ((), (), s32[]{:S(2)}) async-start(), calls=%async_computation.14 | async-start | bytes 1310720 | tf_op jit(solution)/shard_map/all_gather | solution.py:18
  597.5 56.3 %reduce-scatter.8.cloned.1.call-start = ((), (), s32[]{:S(2)}) async-start(), calls=%async_computation.15 | async-start | bytes 1310720 | tf_op jit(solution)/shard_map/reduce_scatter | solution.py:35
  615.0 4.8 copy-start.13
  619.8 34.0 %copy-start.2 = (bf16[256,512]{1,0:T(8,128)(2,1)S(1)}, bf16[256,512]{1,0:T(8,128)(2,1)}, u32[]{:S(2)}) copy-start(bf16[256,512]{1,0:T(8,128)(2,1)} %add_convert_fusion.1) | copy-start | bytes 786436
Sparse Core Ops, SparseCore 0:
  8.9 19.4 all-gather.10
  30.5 92.4 all-gather.12
  125.2 90.4 all-gather.14
  217.7 91.2 all-gather.16
  318.1 22.9 reduce-scatter.3
  343.1 49.1 all-gather.22
  393.8 15.2 all-gather.18
  411.2 49.0 all-gather.24
  462.4 47.6 all-gather.20
  512.0 48.8 all-gather.26
  565.7 22.9 reduce-scatter.5
  597.6 17.3 all-gather.28
  629.0 24.7 reduce-scatter.7
where the time goes:
time: 670 us; the launch traced here: 669 us
  waiting for transfers between devices  536 us (80%)
  blocking collectives  56.8 us (8%)
  matrix products  37.3 us (6%)
  other arithmetic  16.5 us (2%)
  between operations  14.8 us (2%)
  local copies, waits for them, and re-layouts  7.65 us (1%)
    all_gather x1, waiting for transfers between devices, shards(): kept_down = lax.all_gather(down_low, 'fs', axis=1, tiled=True)  93.2 us
    all_gather x1, waiting for transfers between devices, shards(): lax.all_gather(up_low, 'fs', axis=0, tiled=True)  87.9 us
    all_gather x1, waiting for transfers between devices, shards(): lax.all_gather(gate_low, 'fs', axis=0, tiled=True)  68.3 us
    reduce_scatter x3, waiting for transfers between devices, spread_back(): lax.psum_scatter(lax.dot_general(weight_cols, left_rows, (((0,), (1,)), (...  65.6 us
    all_gather x1, waiting for transfers between devices, shards(): lax.all_gather(mixout_weight.astype(jnp.bfloat16), 'fs', axis=1, tiled=True)  50.8 us
    all_gather x1, waiting for transfers between devices, shards(): lax.all_gather(value_weight.astype(jnp.bfloat16), 'fs', axis=0, tiled=True)  48.5 us
    all_gather x1, waiting for transfers between devices, shards(): lax.all_gather(bgate_low, 'fs', axis=0, tiled=True)  47.3 us
    unnamed x1, blocking collectives  39.5 us
  transfers between devices with their start and end apart: 13, of which 12 were waited for; matrix products, arithmetic and copies ran while one was open for 4% of the time, Pallas kernels for 0%

commit v1 on v0

--- a/solution.py
+++ b/solution.py
@@ -8,6 +8,17 @@
 RESIDUAL_SCALE = 1.4142135623730951
 HALF_STEP = 0.5
 EPSILON = 1e-05
+
+
+def turned_line(x, name, along):
+    peers = lax.axis_size(name)
+    right = [(i, (i + 1) % peers) for i in range(peers)]
+    pieces = [x]
+    for reach in range(1, peers):
+        pieces = [lax.ppermute(pieces[0], name, right), *pieces]
+    whole = jnp.concatenate(pieces, axis=along)
+    turn = (lax.axis_index(name) + 1) * pieces[-1].shape[along]
+    return jnp.roll(whole, turn, axis=along)
 
 
 def add_rows(gathered, shard_piece):
@@ -94,7 +105,7 @@
         lax.all_gather(gate_low, "fs", axis=0, tiled=True),
         lax.all_gather(up_low, "fs", axis=0, tiled=True),
     )
-    kept_down = lax.all_gather(down_low, "fs", axis=1, tiled=True)
+    kept_down = turned_line(down_low, "fs", 1)
 
     def channel_mix(gathered):
         gate_sum = jnp.dot(gathered, kept_gate, preferred_element_type=jnp.float32)

time: 670 us -> 648 us (0.967)
  waiting for transfers between devices: 536 us -> 461 us
  local copies, waits for them, and re-layouts: 7.65 us -> 31.4 us
  blocking collectives: 56.8 us -> 78.6 us
    ppermute x0 -> x7, waiting for transfers between devices: none -> 169 us  [turned_line(): pieces = [lax.ppermute(pieces[0], name, right), *pieces]]
    all_gather x1 -> x0, waiting for transfers between devices: 93.2 us -> none  [shards(): kept_down = lax.all_gather(down_low, 'fs', axis=1, tiled=True)]
    all_gather x1, waiting for transfers between devices: 87.9 us -> 5.47 us  [shards(): lax.all_gather(up_low, 'fs', axis=0, tiled=True)]
    all_gather x1, waiting for transfers between devices: 68.3 us -> 0.01 us  [shards(): lax.all_gather(gate_low, 'fs', axis=0, tiled=True)]
    unnamed x55 -> x76, local copies, waits for them, and re-layouts: 2.14 us -> 25.1 us
    unnamed x1, blocking collectives: 39.5 us -> 61.3 us
  transfers between devices with their start and end apart: 13 -> 19, of which waited for: 12 -> 16; matrix products, arithmetic and copies ran while one was open for 4% -> 8% of each run, Pallas kernels for 0% -> 0%
where the time goes in v1:
time: 648 us; the launch traced here: 647 us
  waiting for transfers between devices  461 us (71%)
  blocking collectives  78.6 us (12%)
  matrix products  39.5 us (6%)
  local copies, waits for them, and re-layouts  31.4 us (5%)
  other arithmetic  18.3 us (3%)
  between operations  15.1 us (2%)
    ppermute x7, waiting for transfers between devices, turned_line(): pieces = [lax.ppermute(pieces[0], name, right), *pieces]  169 us
    reduce_scatter x3, waiting for transfers between devices, spread_back(): lax.psum_scatter(lax.dot_general(weight_cols, left_rows, (((0,), (1,)), (...  65.6 us
    unnamed x1, blocking collectives  61.3 us
    all_gather x1, waiting for transfers between devices, shards(): lax.all_gather(mixout_weight.astype(jnp.bfloat16), 'fs', axis=1, tiled=True)  51 us
    all_gather x1, waiting for transfers between devices, shards(): lax.all_gather(value_weight.astype(jnp.bfloat16), 'fs', axis=0, tiled=True)  48.5 us
    all_gather x1, waiting for transfers between devices, shards(): lax.all_gather(bgate_low, 'fs', axis=0, tiled=True)  46.9 us
    all_gather x1, waiting for transfers between devices, shards(): lax.all_gather(cgate_weight.astype(jnp.bfloat16), 'fs', axis=0, tiled=True)  38.6 us
    all_gather x3, waiting for transfers between devices, features(): return lax.all_gather(inputs, 'tp', axis=1, tiled=True)  34.1 us
  transfers between devices with their start and end apart: 19, of which 16 were waited for; matrix products, arithmetic and copies ran while one was open for 8% of the time, Pallas kernels for 0%

profile of v1, /device:TPU:0, one launch (start us, length us, event | category | flops | bytes accessed | tf_op | source)
XLA Modules:
  0.0 647.3 jit_solution(454245976178435187)
XLA Ops:
  7.4 2.3 convert_element_type.73
  9.7 1.4 convert_element_type.72
  11.2 3.0 collective-permute-start
  14.2 0.9 convert_element_type.74
  15.3 18.1 %collective-permute-done = bf16[1408,256]{1,0:T(8,128)(2,1)S(1)} collective-permute-done((bf16[1408,256]{1,0:T(8,128)(2,1)S(1)}, bf16[1408,256]{1,0:T(8,128)(2,1)S(1)}, u32[]{:S(2)}, u32[]{:S(2)}) %collective-permute-start) | collective-permute-done | bytes 720928 | tf_op jit(solution)/shard_map/ppermute | solution.py:18
  33.4 30.5 %collective-permute-done.1 = bf16[1408,256]{1,0:T(8,128)(2,1)S(1)} collective-permute-done((bf16[1408,256]{1,0:T(8,128)(2,1)S(1)}, bf16[1408,256]{1,0:T(8,128)(2,1)S(1)}, u32[]{:S(2)}, u32[]{:S(2)}) %collective-permute-start.1) | collective-permute-done | bytes 720928 | tf_op jit(solution)/shard_map/ppermute | solution.py:18
  63.9 28.2 %collective-permute-done.2 = bf16[1408,256]{1,0:T(8,128)(2,1)S(1)} collective-permute-done((bf16[1408,256]{1,0:T(8,128)(2,1)S(1)}, bf16[1408,256]{1,0:T(8,128)(2,1)S(1)}, u32[]{:S(2)}, u32[]{:S(2)}) %collective-permute-start.2) | collective-permute-done | bytes 720928 | tf_op jit(solution)/shard_map/ppermute | solution.py:18
  92.1 0.9 copy-done.4
  93.0 36.2 %collective-permute-done.3 = bf16[1408,256]{1,0:T(8,128)(2,1)S(1)} collective-permute-done((bf16[1408,256]{1,0:T(8,128)(2,1)S(1)}, bf16[1408,256]{1,0:T(8,128)(2,1)S(1)}, u32[]{:S(2)}, u32[]{:S(2)}) %collective-permute-start.3) | collective-permute-done | bytes 720928 | tf_op jit(solution)/shard_map/ppermute | solution.py:18
  129.2 0.9 copy-done.6
  130.1 36.1 %collective-permute-done.4 = bf16[1408,256]{1,0:T(8,128)(2,1)} collective-permute-done((bf16[1408,256]{1,0:T(8,128)(2,1)S(1)}, bf16[1408,256]{1,0:T(8,128)(2,1)}, u32[]{:S(2)}, u32[]{:S(2)}) %collective-permute-start.4) | collective-permute-done | bytes 720928 | tf_op jit(solution)/shard_map/ppermute | solution.py:18
  167.5 20.3 %collective-permute-done.5 = bf16[1408,256]{1,0:T(8,128)(2,1)} collective-permute-done((bf16[1408,256]{1,0:T(8,128)(2,1)}, bf16[1408,256]{1,0:T(8,128)(2,1)}, u32[]{:S(2)}, u32[]{:S(2)}) %collective-permute-start.5) | collective-permute-done | bytes 720928 | tf_op jit(solution)/shard_map/ppermute | solution.py:18
  189.5 61.3 %all-reduce.8 = (f32[1408]{0:T(1024)S(1)}, f32[1408]{0:T(1024)S(1)}, f32[512]{0:T(512)S(1)}, f32[512]{0:T(512)S(1)}, f32[512]{0:T(512)S(1)}, /*index=5*/f32[512]{0:T(512)S(1)}, f32[512]{0:T(512)S(1)}) all-reduce(f32[1408]{0:T(1024)S(1)} %dynamic-update-slice, f32[1408]{0:T(1024)S(1)} %dynamic-update-slice.1, ...), channel_id=1, replica_groups=mesh['fs'=8,'tp'=4] {'fs'}, use_global_device_ids=true, to_apply=%add.1 | all-reduce | flops 5376 | bytes 43008
  250.8 2.2 constant_dynamic-update-slice_fusion.15
  253.0 2.1 constant_dynamic-update-slice_fusion.14
  255.1 2.1 constant_dynamic-update-slice_fusion.13
  257.2 2.1 constant_dynamic-update-slice_fusion.12
  259.3 1.0 constant_dynamic-update-slice_fusion.11
  260.3 1.0 constant_dynamic-update-slice_fusion.10
  261.3 1.0 constant_dynamic-update-slice_fusion.9
  262.2 1.0 constant_dynamic-update-slice_fusion.8
  263.3 2.1 constant_dynamic-update-slice_fusion.7
  265.3 2.1 constant_dynamic-update-slice_fusion.6
  267.4 2.1 constant_dynamic-update-slice_fusion.5
  269.6 1.0 constant_dynamic-update-slice_fusion.4
  270.5 1.0 constant_dynamic-update-slice_fusion.3
  271.5 1.0 constant_dynamic-update-slice_fusion.2
  272.5 1.0 constant_dynamic-update-slice_fusion.1
  273.4 0.9 constant_dynamic-update-slice_fusion
  274.4 5.9 convolution_multiply_fusion.3
  280.3 5.5 all-gather.14.cloned.1.call-done
  285.8 9.6 %fusion.6 = bf16[2048,256]{1,0:T(8,128)(2,1)} fusion(bf16[1408,4096]{1,0:T(8,128)(2,1)} %constant_dynamic-update-slice_fusion, s32[]{:T(128)S(6)} %select_n.23, bf16[256,2048]{1,0:T(8,128)(2,1)} %all-gather.10.cloned.1.call-done, bf16[2048,1408]{1,0:T(8,128)(2,1)} %all-gather.14.cloned.1.call-done, f32[256,1408]{1,0:T(8,128)} %convolution_multiply_fusion.3, ...), kind=kOutput, calls=%fused_computation.11 | convolution fusion | flops 2955837440 | bytes 15078916 | tf_op jit(solution)/shard_map/dot_general | solution.py:47
  295.4 0.8 convert_element_type.81
  296.4 0.8 dynamic_slice.26
  297.2 0.8 dynamic_slice.27
  297.9 20.7 %reduce-scatter.4.cloned.1.call-done = bf16[512,256]{1,0:T(8,128)(2,1)} async-done(((bf16[2048,256]{1,0:T(8,128)(2,1)}), bf16[512,256]{1,0:T(8,128)(2,1)}) %reduce-scatter.4.cloned.1.call-update) | async-done | bytes 262160 | tf_op jit(solution)/shard_map/reduce_scatter | solution.py:46
  318.6 1.2 fusion.23
  319.8 5.8 all-reduce.11
  325.5 1.9 add_convert_fusion.2
  330.2 0.9 constant_dynamic-slice_fusion
  331.1 38.6 %all-gather.20.cloned.1.call-done = bf16[2048,512]{1,0:T(8,128)(2,1)} async-done(((bf16[256,512]{1,0:T(8,128)(2,1)}), bf16[2048,512]{1,0:T(8,128)(2,1)}) %all-gather.20.cloned.1.call-update) | async-done | bytes 2097168 | tf_op jit(solution)/shard_map/all_gather | solution.py:124
  369.7 16.7 %all-gather.16.cloned.1.call-done = bf16[256,2048]{0,1:T(8,128)(2,1)} async-done(((bf16[256,512]{0,1:T(8,128)(2,1)}), bf16[256,2048]{0,1:T(8,128)(2,1)}) %all-gather.16.cloned.1.call-update) | async-done | bytes 1048592 | tf_op jit(solution)/shard_map/all_gather | solution.py:29
  386.4 2.7 convolution_multiply_fusion.5
  389.1 48.5 %all-gather.22.cloned.1.call-done = bf16[2048,512]{1,0:T(8,128)(2,1)} async-done(((bf16[256,512]{1,0:T(8,128)(2,1)}), bf16[2048,512]{1,0:T(8,128)(2,1)}) %all-gather.22.cloned.1.call-update) | async-done | bytes 2097168 | tf_op jit(solution)/shard_map/all_gather | solution.py:127
  437.6 2.7 fusion.15
  440.5 46.9 %all-gather.18.cloned.1.call-done = bf16[2048,512]{1,0:T(8,128)(2,1)} async-done(((bf16[256,512]{1,0:T(8,128)(2,1)}), bf16[2048,512]{1,0:T(8,128)(2,1)}) %all-gather.18.cloned.1.call-update) | async-done | bytes 2097168 | tf_op jit(solution)/shard_map/all_gather | solution.py:122
  487.4 51.0 %all-gather.24.cloned.1.call-done = bf16[512,2048]{1,0:T(8,128)(2,1)} async-done(((bf16[512,256]{1,0:T(8,128)(2,1)}), bf16[512,2048]{1,0:T(8,128)(2,1)}) %all-gather.24.cloned.1.call-update) | async-done | bytes 2097168 | tf_op jit(solution)/shard_map/all_gather | solution.py:136
  538.3 4.6 fusion.14
  543.1 0.8 dynamic_slice.29
  543.8 0.8 dynamic_slice.30
  544.6 21.5 %reduce-scatter.6.cloned.1.call-done = bf16[512,256]{1,0:T(8,128)(2,1)} async-done(((bf16[2048,256]{1,0:T(8,128)(2,1)}), bf16[512,256]{1,0:T(8,128)(2,1)}) %reduce-scatter.6.cloned.1.call-update) | async-done | bytes 262160 | tf_op jit(solution)/shard_map/reduce_scatter | solution.py:46
  566.1 1.1 fusion.22
  567.3 5.8 all-reduce.10
  573.1 1.9 add_convert_fusion.1
  575.1 17.4 %all-gather.26.cloned.1.call-done = bf16[256,2048]{0,1:T(8,128)(2,1)} async-done(((bf16[256,512]{0,1:T(8,128)(2,1)}), bf16[256,2048]{0,1:T(8,128)(2,1)}) %all-gather.26.cloned.1.call-update) | async-done | bytes 1048592 | tf_op jit(solution)/shard_map/all_gather | solution.py:29
  592.5 4.9 convolution_multiply_fusion.1
  597.4 9.1 %fusion.9 = bf16[2048,256]{1,0:T(8,128)(2,1)} fusion(bf16[1408,4096]{1,0:T(8,128)(2,1)} %constant_dynamic-update-slice_fusion, s32[]{:T(128)S(6)} %select_n.23, bf16[256,2048]{0,1:T(8,128)(2,1)S(1)} %copy-done.3, bf16[2048,1408]{1,0:T(8,128)(2,1)} %all-gather.14.cloned.1.call-done, f32[256,1408]{1,0:T(8,128)S(1)} %convolution_multiply_fusion.1, ...), kind=kOutput, calls=%fused_computation.12 | convolution fusion | flops 2955837440 | bytes 15078916 | tf_op jit(solution)/shard_map/dot_general | solution.py:47
  606.5 0.8 dynamic_slice.31
  607.3 0.8 dynamic_slice.32
  608.0 23.4 %reduce-scatter.8.cloned.1.call-done = bf16[512,256]{1,0:T(8,128)(2,1)} async-done(((bf16[2048,256]{1,0:T(8,128)(2,1)}), bf16[512,256]{1,0:T(8,128)(2,1)}) %reduce-scatter.8.cloned.1.call-update) | async-done | bytes 262160 | tf_op jit(solution)/shard_map/reduce_scatter | solution.py:46
  631.5 1.2 fusion.24
  632.6 5.8 all-reduce.9
  638.4 1.2 add_convert_fusion
  639.6 0.8 copy.25
  (100 shorter events, 5.8 us)
Async XLA Ops:
  6.5 159.6 %copy-start.22 = (u32[32]{0:T(128)S(1)}, u32[32]{0:T(128)}, u32[]{:S(2)}) copy-start(u32[32]{0:T(128)} %constant.71) | copy-start | bytes 388
  6.5 7.7 %copy-start.8 = (f32[256,1408]{1,0:T(8,128)S(1)}, f32[256,1408]{1,0:T(8,128)}, u32[]{:S(2)}) copy-start(f32[256,1408]{1,0:T(8,128)} %param.24) | copy-start | bytes 4325380
  6.5 160.9 %copy-start.17 = (f32[1,64]{1,0:T(1,128)S(1)}, f32[1,64]{1,0:T(1,128)}, u32[]{:S(2)}) copy-start(f32[1,64]{1,0:T(1,128)} %param.37) | copy-start | bytes 772
  6.5 181.3 %copy-start.18 = (f32[1,64]{1,0:T(1,128)S(1)}, f32[1,64]{1,0:T(1,128)}, u32[]{:S(2)}) copy-start(f32[1,64]{1,0:T(1,128)} %param.34) | copy-start | bytes 772
  6.5 182.1 %copy-start.14 = (f32[1,176]{1,0:T(1,128)S(1)}, f32[1,176]{1,0:T(1,128)}, u32[]{:S(2)}) copy-start(f32[1,176]{1,0:T(1,128)} %param.26) | copy-start | bytes 2116
  6.5 182.4 %copy-start.15 = (f32[1,176]{1,0:T(1,128)S(1)}, f32[1,176]{1,0:T(1,128)}, u32[]{:S(2)}) copy-start(f32[1,176]{1,0:T(1,128)} %param.27) | copy-start | bytes 2116
  6.6 182.6 %copy-start.19 = (f32[1,64]{1,0:T(1,128)S(1)}, f32[1,64]{1,0:T(1,128)}, u32[]{:S(2)}) copy-start(f32[1,64]{1,0:T(1,128)} %param.33) | copy-start | bytes 772
  6.6 182.7 %copy-start.20 = (f32[1,64]{1,0:T(1,128)S(1)}, f32[1,64]{1,0:T(1,128)}, u32[]{:S(2)}) copy-start(f32[1,64]{1,0:T(1,128)} %param.32) | copy-start | bytes 772
  6.6 182.8 %copy-start.21 = (f32[1,64]{1,0:T(1,128)S(1)}, f32[1,64]{1,0:T(1,128)}, u32[]{:S(2)}) copy-start(f32[1,64]{1,0:T(1,128)} %param.28) | copy-start | bytes 772
  6.6 267.8 %all-gather.10.cloned.1.call-start = ((), (), s32[]{:S(2)}) async-start(), calls=%async_computation.3 | async-start | bytes 1310720 | tf_op jit(solution)/shard_map/all_gather | solution.py:29
  7.3 267.1 %all-gather.12.cloned.1.call-start = ((), (), s32[]{:S(2)}) async-start(), calls=%async_computation.4 | async-start | bytes 6488064 | tf_op jit(solution)/shard_map/all_gather | solution.py:105
  9.7 276.1 %all-gather.14.cloned.1.call-start = ((), (), s32[]{:S(2)}) async-start(), calls=%async_computation.5 | async-start | bytes 6488064 | tf_op jit(solution)/shard_map/all_gather | solution.py:106
  11.2 22.2 %collective-permute-start = (bf16[1408,256]{1,0:T(8,128)(2,1)S(1)}, bf16[1408,256]{1,0:T(8,128)(2,1)S(1)}, u32[]{:S(2)}, u32[]{:S(2)}) collective-permute-start(bf16[1408,256]{1,0:T(8,128)(2,1)S(1)} %convert_element_type.72), channel_id=1, source_target_pairs={{0,4},{4,8},{8,12},{12,16},{16,20},{20,24},{24,28},{28,0},{1,5},{5... | collective-permute-start | bytes 2162696 | tf_op jit(solution)/shard_map/ppermute | solution.py:18
  15.2 247.0 %copy-start = (f32[1408,256]{1,0:T(8,128)S(1)}, f32[1408,256]{1,0:T(8,128)}, u32[]{:S(2)}) copy-start(f32[1408,256]{1,0:T(8,128)} %param.25) | copy-start | bytes 4325380
  15.2 303.4 %reduce-scatter.4.cloned.1.call-start = ((), (), s32[]{:S(2)}) async-start(), calls=%async_computation.6 | async-start | bytes 1310720 | tf_op jit(solution)/shard_map/reduce_scatter | solution.py:46
  33.4 30.5 %collective-permute-start.1 = (bf16[1408,256]{1,0:T(8,128)(2,1)S(1)}, bf16[1408,256]{1,0:T(8,128)(2,1)S(1)}, u32[]{:S(2)}, u32[]{:S(2)}) collective-permute-start(bf16[1408,256]{1,0:T(8,128)(2,1)S(1)} %collective-permute-done), channel_id=1, source_target_pairs={{0,4},{4,8},{8,12},{12,16},{16,20},{20,24},{24,28},{28,0},{1,5},{5... | collective-permute-start | bytes 2162696 | tf_op jit(solution)/shard_map/ppermute | solution.py:18
  63.9 28.2 %collective-permute-start.2 = (bf16[1408,256]{1,0:T(8,128)(2,1)S(1)}, bf16[1408,256]{1,0:T(8,128)(2,1)S(1)}, u32[]{:S(2)}, u32[]{:S(2)}) collective-permute-start(bf16[1408,256]{1,0:T(8,128)(2,1)S(1)} %collective-permute-done.1), channel_id=1, source_target_pairs={{0,4},{4,8},{8,12},{12,16},{16,20},{20,24},{24,28},{28,0},{1,5},{5... | collective-permute-start | bytes 2162696 | tf_op jit(solution)/shard_map/ppermute | solution.py:18
  92.1 0.9 copy-start.4
  93.0 36.2 %collective-permute-start.3 = (bf16[1408,256]{1,0:T(8,128)(2,1)S(1)}, bf16[1408,256]{1,0:T(8,128)(2,1)S(1)}, u32[]{:S(2)}, u32[]{:S(2)}) collective-permute-start(bf16[1408,256]{1,0:T(8,128)(2,1)S(1)} %collective-permute-done.2), channel_id=1, source_target_pairs={{0,4},{4,8},{8,12},{12,16},{16,20},{20,24},{24,28},{28,0},{1,5},{5... | collective-permute-start | bytes 2162696 | tf_op jit(solution)/shard_map/ppermute | solution.py:18
  129.2 0.9 copy-start.6
  130.1 36.1 %collective-permute-start.4 = (bf16[1408,256]{1,0:T(8,128)(2,1)S(1)}, bf16[1408,256]{1,0:T(8,128)(2,1)}, u32[]{:S(2)}, u32[]{:S(2)}) collective-permute-start(bf16[1408,256]{1,0:T(8,128)(2,1)S(1)} %collective-permute-done.3), channel_id=1, source_target_pairs={{0,4},{4,8},{8,12},{12,16},{16,20},{20,24},{24,28},{28,0},{1,5},{5... | collective-permute-start | bytes 2162696 | tf_op jit(solution)/shard_map/ppermute | solution.py:18
  166.2 21.7 %collective-permute-start.5 = (bf16[1408,256]{1,0:T(8,128)(2,1)}, bf16[1408,256]{1,0:T(8,128)(2,1)}, u32[]{:S(2)}, u32[]{:S(2)}) collective-permute-start(bf16[1408,256]{1,0:T(8,128)(2,1)} %collective-permute-done.4), channel_id=1, source_target_pairs={{0,4},{4,8},{8,12},{12,16},{16,20},{20,24},{24,28},{28,0},{1,5},{5... | collective-permute-start | bytes 2162696 | tf_op jit(solution)/shard_map/ppermute | solution.py:18
  187.8 63.0 %collective-permute-start.6 = (bf16[1408,256]{1,0:T(8,128)(2,1)}, bf16[1408,256]{1,0:T(8,128)(2,1)}, u32[]{:S(2)}, u32[]{:S(2)}) collective-permute-start(bf16[1408,256]{1,0:T(8,128)(2,1)} %collective-permute-done.5), channel_id=1, source_target_pairs={{0,4},{4,8},{8,12},{12,16},{16,20},{20,24},{24,28},{28,0},{1,5},{5... | collective-permute-start | bytes 2162696 | tf_op jit(solution)/shard_map/ppermute | solution.py:18
  250.8 8.4 %copy-start.5 = (bf16[1408,256]{1,0:T(8,128)(2,1)S(1)}, bf16[1408,256]{1,0:T(8,128)(2,1)}, u32[]{:S(2)}) copy-start(bf16[1408,256]{1,0:T(8,128)(2,1)} %copy-done.4) | copy-start | bytes 2162692
  259.3 10.3 %copy-start.7 = (bf16[1408,256]{1,0:T(8,128)(2,1)S(1)}, bf16[1408,256]{1,0:T(8,128)(2,1)}, u32[]{:S(2)}) copy-start(bf16[1408,256]{1,0:T(8,128)(2,1)} %copy-done.6) | copy-start | bytes 2162692
  285.7 9.7 %copy-start.10 = (f32[256,512]{1,0:T(8,128)S(1)}, f32[256,512]{1,0:T(8,128)}, u32[]{:S(2)}) copy-start(f32[256,512]{1,0:T(8,128)} %param.30) | copy-start | bytes 1572868
  285.7 10.5 %copy-start.9 = (bf16[256,512]{1,0:T(8,128)(2,1)S(1)}, bf16[256,512]{1,0:T(8,128)(2,1)}, u32[]{:S(2)}) copy-start(bf16[256,512]{1,0:T(8,128)(2,1)} %param.22) | copy-start | bytes 786436
  285.8 41.8 %copy-start.11 = (f32[256,512]{1,0:T(8,128)S(1)}, f32[256,512]{1,0:T(8,128)}, u32[]{:S(2)}) copy-start(f32[256,512]{1,0:T(8,128)} %param.31) | copy-start | bytes 1572868
  285.8 42.6 %copy-start.12 = (f32[256,512]{1,0:T(8,128)S(1)}, f32[256,512]{1,0:T(8,128)}, u32[]{:S(2)}) copy-start(f32[256,512]{1,0:T(8,128)} %param.29) | copy-start | bytes 1572868
  295.3 33.8 %copy-start.13 = (f32[512,256]{1,0:T(8,128)S(1)}, f32[512,256]{1,0:T(8,128)}, u32[]{:S(2)}) copy-start(f32[512,256]{1,0:T(8,128)} %param.36) | copy-start | bytes 1572868
  295.4 74.3 %all-gather.20.cloned.1.call-start = ((), (), s32[]{:S(2)}) async-start(), calls=%async_computation.9 | async-start | bytes 2359296 | tf_op jit(solution)/shard_map/all_gather | solution.py:124
  296.2 90.2 %all-gather.16.cloned.1.call-start = ((), (), s32[]{:S(2)}) async-start(), calls=%async_computation.7 | async-start | bytes 1310720 | tf_op jit(solution)/shard_map/all_gather | solution.py:29
  327.5 110.1 %all-gather.22.cloned.1.call-start = ((), (), s32[]{:S(2)}) async-start(), calls=%async_computation.10 | async-start | bytes 2359296 | tf_op jit(solution)/shard_map/all_gather | solution.py:127
  328.3 159.1 %all-gather.18.cloned.1.call-start = ((), (), s32[]{:S(2)}) async-start(), calls=%async_computation.8 | async-start | bytes 2359296 | tf_op jit(solution)/shard_map/all_gather | solution.py:122
  329.1 209.2 %all-gather.24.cloned.1.call-start = ((), (), s32[]{:S(2)}) async-start(), calls=%async_computation.11 | async-start | bytes 2359296 | tf_op jit(solution)/shard_map/all_gather | solution.py:136
  329.9 236.2 %reduce-scatter.6.cloned.1.call-start = ((), (), s32[]{:S(2)}) async-start(), calls=%async_computation.12 | async-start | bytes 1310720 | tf_op jit(solution)/shard_map/reduce_scatter | solution.py:46
  386.4 152.0 %copy-start.16 = (bf16[256,2048]{0,1:T(8,128)(2,1)S(1)}, bf16[256,2048]{0,1:T(8,128)(2,1)}, u32[]{:S(2)}) copy-start(bf16[256,2048]{0,1:T(8,128)(2,1)} %all-gather.16.cloned.1.call-done) | copy-start | bytes 3145732
  437.6 128.5 %copy-start.1 = (bf16[256,512]{0,1:T(8,128)(2,1)S(1)}, bf16[256,512]{0,1:T(8,128)(2,1)}, u32[]{:S(2)}) copy-start(bf16[256,512]{0,1:T(8,128)(2,1)} %add_convert_fusion.2) | copy-start | bytes 786436
  543.0 49.5 %all-gather.26.cloned.1.call-start = ((), (), s32[]{:S(2)}) async-start(), calls=%async_computation.13 | async-start | bytes 1310720 | tf_op jit(solution)/shard_map/all_gather | solution.py:29
  575.0 56.4 %reduce-scatter.8.cloned.1.call-start = ((), (), s32[]{:S(2)}) async-start(), calls=%async_computation.14 | async-start | bytes 1310720 | tf_op jit(solution)/shard_map/reduce_scatter | solution.py:46
  592.5 4.9 copy-start.3
  597.4 34.1 %copy-start.2 = (bf16[256,512]{0,1:T(8,128)(2,1)S(1)}, bf16[256,512]{0,1:T(8,128)(2,1)}, u32[]{:S(2)}) copy-start(bf16[256,512]{0,1:T(8,128)(2,1)} %add_convert_fusion.1) | copy-start | bytes 786436
Sparse Core Ops, SparseCore 0:
  9.0 19.4 all-gather.9
  30.6 133.5 all-gather.11
  166.4 119.2 all-gather.13
  295.5 23.0 reduce-scatter.3
  320.6 49.0 all-gather.19
  371.1 15.2 all-gather.15
  388.5 49.0 all-gather.21
  439.7 47.6 all-gather.17
  489.4 48.8 all-gather.23
  543.1 22.9 reduce-scatter.5
  575.1 17.3 all-gather.25
  606.6 24.7 reduce-scatter.7
